TPU v7x, 32 devices: a whole 2x2x4 slice. The times are simulated.
32 devices in a mesh: ep: 8 (over z, y), tp: 4 (over x, core).
Axes of the slice: x: 2, y: 2, z: 4, core: 2. Of those that a mesh axis runs over, the one named last changes fastest.
Arguments:
- mix_tokens: bfloat16 [8192, 2048], P(('ep', 'tp')), may hold values from -6 to 6
- mix_gain: bfloat16 [2048], replicated, may hold values from 0.099609375 to 1.8984375
- w_branch: bfloat16 [2048, 2048], P(None, 'tp'), may hold values from -0.125 to 0.125
- w_gate_branch: bfloat16 [2048, 2048], P(None, 'tp'), may hold values from -0.125 to 0.125
- conv_taps: bfloat16 [4, 2048], P(None, 'tp'), may hold values from -3 to 3
- recur_gate_w: bfloat16 [32, 64, 64], P('tp'), may hold values from -0.75 to 0.75
- inject_gate_w: bfloat16 [32, 64, 64], P('tp'), may hold values from -0.75 to 0.75
- decay_logit: float32 [2048], P('tp')
- decay_kick: float32 [8192, 32], P('ep', 'tp'), may hold values from -0.7 to 0
- w_mix_out: bfloat16 [2048, 2048], P('tp'), may hold values from -0.125 to 0.125
- moe_tokens: bfloat16 [4096, 2048], P(('ep', 'tp')), may hold values from -6 to 6
- moe_gain: bfloat16 [2048], replicated, may hold values from 0.099609375 to 1.8984375
- expert_ids: int32 [4096, 2], P(('ep', 'tp')), may hold values from 0 to 7, all different within a row; in each aligned block of 128 rows (0 to 127, 128 to 255, ...) at most 64 rows name the same one
- route_weight: float32 [4096, 2], P(('ep', 'tp')), may hold values from 0.1 to 1
- expert_gate_w: bfloat16 [8, 2048, 1024], P('ep', None, 'tp'), may hold values from -0.125 to 0.125
- expert_up_w: bfloat16 [8, 2048, 1024], P('ep', None, 'tp'), may hold values from -0.125 to 0.125
- expert_down_w: bfloat16 [8, 1024, 2048], P('ep', 'tp'), may hold values from -0.1875 to 0.1875
Outputs:
- mixer_out: bfloat16 [8192, 2048], P(('ep', 'tp'))
- expert_out: bfloat16 [4096, 2048], P(('ep', 'tp'))
Inputs may be any that keep to these rules, and one draw needn't show every extreme that they name: `expert_ids`: each row names 2 different experts. In each aligned block of 128 rows (the rows of one device) no expert is named more than 64 times, a bound that some block reaches.
All inputs are finite; a program needn't handle non-finite values.
Results may differ from a plain program's by a relative error of at most 0.015.
Values may be sent and summed in bfloat16 or wider, within the bound.
A program may use at most 128 MiB of HBM per device.

v0:
```python
import jax
import jax.numpy as jnp
from jax import lax
from jax.sharding import PartitionSpec as P

epsilon = 1e-06
gate_const = 8.0


def from_behind(block, axis, distance):
    devices = range(lax.axis_size(axis))
    route = [(i - distance, i) for i in devices if i - distance in devices]
    return lax.ppermute(block, axis, route)


def entering(part, axis, combine, identity):
    place = lax.axis_index(axis)
    gathered = jax.tree.map(lambda a: lax.all_gather(a, axis), part)
    state = jax.tree.map(lambda a, e: jnp.zeros_like(a) + jnp.asarray(e, a.dtype), part, identity)

    def one(step, state):
        return combine(
            state, jax.tree.map(lambda a: lax.dynamic_index_in_dim(a, step, 0, False), gathered)
        )

    return lax.fori_loop(0, place, one, state)


def norm_rows(values, gain_vec):
    value_f32 = values.astype(jnp.float32)
    inv_scale = lax.rsqrt(jnp.mean(value_f32 * value_f32, axis=-1, keepdims=True) + epsilon)
    return (value_f32 * inv_scale * gain_vec.astype(jnp.float32)).astype(jnp.bfloat16)


def chain_link(earlier, later):
    return (later[0] * earlier[0], later[0] * earlier[1] + later[1])


def block_diagonal(head_maps):
    head_count, head_dim, _ = head_maps.shape
    head_eye = jnp.eye(head_count, dtype=head_maps.dtype)
    spread = head_maps[:, :, None, :] * head_eye[:, None, :, None]
    return spread.reshape(head_count * head_dim, head_count * head_dim)


def run_mixer(
    mix_tokens,
    mix_gain,
    w_branch,
    w_gate_branch,
    conv_taps,
    recur_gate_w,
    inject_gate_w,
    decay_logit,
    decay_kick,
    w_mix_out,
):
    mixer_in = norm_rows(mix_tokens, mix_gain)
    col_count = w_branch.shape[1]
    piece = lax.all_gather(mixer_in, "tp", axis=0, tiled=True)
    first = jnp.dot(piece, w_branch, preferred_element_type=jnp.float32).astype(jnp.bfloat16)
    second = jnp.dot(piece, w_gate_branch, preferred_element_type=jnp.float32).astype(jnp.bfloat16)
    both_proj = jnp.stack([first, second], axis=0)
    branch_x = both_proj[0]
    branch_gate = both_proj[1]
    row_count = branch_x.shape[0]
    tap_count = conv_taps.shape[0]
    rim_rows = from_behind(branch_x[row_count - (tap_count - 1) :], "ep", 1)
    extended = jnp.concatenate([rim_rows, branch_x], axis=0).astype(jnp.float32)
    tap_values = conv_taps.astype(jnp.float32)
    conv_out = tap_values[tap_count - 1] * extended[tap_count - 1 :]
    for index_value in range(tap_count - 1):
        conv_out = (
            conv_out + tap_values[index_value] * extended[index_value : index_value + row_count]
        )
    conv_low = conv_out.astype(jnp.bfloat16)
    head_count = recur_gate_w.shape[0]
    head_dim = recur_gate_w.shape[1]
    gate_maps = jnp.concatenate(
        [block_diagonal(recur_gate_w), block_diagonal(inject_gate_w)], axis=1
    )
    gate_pre = jnp.dot(conv_low, gate_maps, preferred_element_type=jnp.float32)
    recur = jax.nn.sigmoid(gate_pre[:, :col_count])
    inject = jax.nn.sigmoid(gate_pre[:, col_count:])
    slowness = jax.nn.softplus(-decay_logit)
    widen = (
        jnp.arange(col_count, dtype=jnp.int32)[None, :] // head_dim
        == jnp.arange(head_count, dtype=jnp.int32)[:, None]
    ).astype(jnp.float32)
    kick_wide = jnp.dot(decay_kick, widen, precision=lax.Precision.HIGHEST)
    log_decay = -gate_const * recur * slowness[None, :] + kick_wide
    drive = jnp.sqrt(-jnp.expm1(2.0 * log_decay)) * inject * conv_out
    acc_decay, local_state = lax.associative_scan(chain_link, (jnp.exp(log_decay), drive), axis=0)
    identity = (jnp.ones((col_count,), jnp.float32), jnp.zeros((col_count,), jnp.float32))
    carried = entering(
        (acc_decay[row_count - 1], local_state[row_count - 1]), "ep", chain_link, identity
    )
    state = local_state + acc_decay * carried[1][None, :]
    mixed = (state * jax.nn.gelu(branch_gate.astype(jnp.float32))).astype(jnp.bfloat16)
    return lax.psum_scatter(
        jnp.dot(mixed, w_mix_out, preferred_element_type=jnp.float32).astype(jnp.bfloat16),
        "tp",
        scatter_dimension=0,
        tiled=True,
    )


def run_experts(
    moe_tokens, moe_gain, expert_ids, route_weight, expert_gate_w, expert_up_w, expert_down_w
):
    moe_in = norm_rows(moe_tokens, moe_gain)
    local_rows, top_count = expert_ids.shape
    experts = lax.axis_size("ep")
    room = 2 * local_rows * top_count // experts
    flat_ids = expert_ids.reshape(-1)
    onehot = (flat_ids[:, None] == jnp.arange(experts, dtype=jnp.int32)[None, :]).astype(jnp.int32)
    earlier_count = jnp.cumsum(onehot, axis=0) - onehot
    slot_index = jnp.sum(earlier_count * onehot, axis=1)
    slot_target = flat_ids * room + slot_index
    slots_total = experts * room
    slot_table = (slot_target[:, None] == jnp.arange(slots_total, dtype=jnp.int32)[None, :]).astype(
        jnp.bfloat16
    )
    token_of = (
        jnp.arange(local_rows * top_count, dtype=jnp.int32)[None, :] // top_count
        == jnp.arange(local_rows, dtype=jnp.int32)[:, None]
    ).astype(jnp.bfloat16)
    dispatch_table = jnp.dot(token_of, slot_table, preferred_element_type=jnp.float32).astype(
        jnp.bfloat16
    )
    outgoing = jnp.dot(dispatch_table.T, moe_in, preferred_element_type=jnp.float32).astype(
        jnp.bfloat16
    )
    arrived = lax.all_to_all(outgoing, "ep", split_axis=0, concat_axis=0, tiled=True)
    gate_mat = expert_gate_w[0]
    up_mat = expert_up_w[0]
    down_mat = expert_down_w[0]
    full_gate, full_up, full_down = (
        lax.all_gather(gate_mat, "tp", axis=1, tiled=True),
        lax.all_gather(up_mat, "tp", axis=1, tiled=True),
        lax.all_gather(down_mat, "tp", axis=0, tiled=True),
    )
    hidden = (
        jax.nn.silu(jnp.dot(arrived, full_gate, preferred_element_type=jnp.float32))
        * jnp.dot(arrived, full_up, preferred_element_type=jnp.float32)
    ).astype(jnp.bfloat16)
    groups = lax.axis_size("tp")
    quarter = down_mat.shape[0]
    summed_rows = jnp.zeros((arrived.shape[0], full_down.shape[1]), jnp.float32)
    for group in range(groups):
        piece = jnp.dot(
            hidden[:, group * quarter : (group + 1) * quarter],
            full_down[group * quarter : (group + 1) * quarter],
            preferred_element_type=jnp.float32,
        )
        summed_rows = summed_rows + lax.optimization_barrier(piece.astype(jnp.bfloat16)).astype(
            jnp.float32
        )
    expert_done = summed_rows.astype(jnp.bfloat16)
    returned = lax.all_to_all(expert_done, "ep", split_axis=0, concat_axis=0, tiled=True)
    weighted_table = jnp.zeros((local_rows, slots_total), jnp.float32)
    for pick in range(top_count):
        pick_table = (
            slot_target.reshape(local_rows, top_count)[:, pick][:, None]
            == jnp.arange(slots_total, dtype=jnp.int32)[None, :]
        ).astype(jnp.float32)
        weighted_table = weighted_table + pick_table * route_weight[:, pick][:, None]
    combined = jnp.dot(
        weighted_table, returned.astype(jnp.float32), precision=lax.Precision.HIGHEST
    )
    return combined.astype(jnp.bfloat16)


def body(
    mix_tokens,
    mix_gain,
    w_branch,
    w_gate_branch,
    conv_taps,
    recur_gate_w,
    inject_gate_w,
    decay_logit,
    decay_kick,
    w_mix_out,
    moe_tokens,
    moe_gain,
    expert_ids,
    route_weight,
    expert_gate_w,
    expert_up_w,
    expert_down_w,
):
    mixer_out = run_mixer(
        mix_tokens,
        mix_gain,
        w_branch,
        w_gate_branch,
        conv_taps,
        recur_gate_w,
        inject_gate_w,
        decay_logit,
        decay_kick,
        w_mix_out,
    )
    expert_out = run_experts(
        moe_tokens, moe_gain, expert_ids, route_weight, expert_gate_w, expert_up_w, expert_down_w
    )
    return (mixer_out, expert_out)


def solution(mesh):
    placed = (
        P(("ep", "tp"), None),
        P(),
        P(None, "tp"),
        P(None, "tp"),
        P(None, "tp"),
        P("tp", None, None),
        P("tp", None, None),
        P("tp"),
        P("ep", "tp"),
        P("tp", None),
        P(("ep", "tp"), None),
        P(),
        P(("ep", "tp"), None),
        P(("ep", "tp"), None),
        P("ep", None, "tp"),
        P("ep", None, "tp"),
        P("ep", "tp", None),
    )
    return jax.shard_map(
        body,
        mesh=mesh,
        in_specs=placed,
        out_specs=(P(("ep", "tp"), None), P(("ep", "tp"), None)),
        check_vma=False,
    )
```

profile of v0, /device:TPU:0, one launch (start us, length us, event | category | flops | bytes accessed | tf_op | source)
XLA Modules:
  0.0 439.7 jit_solution(12719589404088025588)
XLA Ops:
  17.9 7.5 %all-to-all-start = ((bf16[8,64,2048]{2,1,0:T(8,128)(2,1)}), bf16[8,64,2048]{2,1,0:T(8,128)(2,1)}, u32[]{:S(2)}, u32[]{:S(2)}) async-start(bf16[8,64,2048]{2,1,0:T(8,128)(2,1)} %bitcast.76), calls=%async_computation.1 | async-start | bytes 4194304 | tf_op jit(solution)/shard_map/all_to_all | solution.py:134
  27.4 22.1 %all-gather.10.cloned.1.call-done = bf16[1024,2048]{1,0:T(8,128)(2,1)} async-done(((bf16[256,2048]{1,0:T(8,128)(2,1)}), bf16[1024,2048]{1,0:T(8,128)(2,1)}) %all-gather.10.cloned.1.call-update) | async-done | bytes 4194320 | tf_op jit(solution)/shard_map/all_gather | solution.py:60
  49.4 5.2 %convolution_convert_fusion.8 = bf16[1024,512]{1,0:T(8,128)(2,1)S(1)} fusion(bf16[1024,2048]{1,0:T(8,128)(2,1)} %all-gather.10.cloned.1.call-done, bf16[2048,512]{1,0:T(8,128)(2,1)} %param.21), kind=kOutput, calls=%fused_computation.52 | convolution fusion | flops 2148007936 | bytes 7340032 | tf_op jit(solution)/shard_map/dot_general | solution.py:61
  67.3 5.1 %fusion.18 = (f32[1024,512]{1,0:T(8,128)}, f32[1024,512]{1,0:T(8,128)}) fusion(f32[1024,512]{1,0:T(8,128)S(1)} %fusion.24, f32[1024,1024]{1,0:T(8,128)S(1)} %fusion.33, f32[1024,8]{0,1:T(8,128)S(1)} %copy-done.54, s32[512]{0:T(512)S(1)} %add_select_fusion, f32[512]{0:T(512)S(1)} %fusion.75), kind=kOutput, calls=%fused_computation.36 | convolution fusion | flops 56627200 | bytes 10522624 | tf_op jit(solution)/shard_map/dot_general | solution.py:90
  72.4 6.3 %slice.385 = f32[512,512]{1,0:T(8,128)} slice(f32[1024,512]{1,0:T(8,128)} %get-tuple-element.59), slice={[0:1023:2], [0:512:1]} | slice | bytes 2097152 | tf_op jit(solution)/shard_map/slice | solution.py:93
  78.7 6.3 %slice.386 = f32[512,512]{1,0:T(8,128)} slice(f32[1024,512]{1,0:T(8,128)} %get-tuple-element.59), slice={[1:1024:2], [0:512:1]} | slice | bytes 2097152 | tf_op jit(solution)/shard_map/slice | solution.py:93
  84.9 6.3 %slice.384 = f32[512,512]{1,0:T(8,128)} slice(f32[1024,512]{1,0:T(8,128)} %get-tuple-element.60), slice={[1:1024:2], [0:512:1]} | slice | bytes 2097152 | tf_op jit(solution)/shard_map/slice | solution.py:93
  91.2 6.3 %slice.388 = f32[512,512]{1,0:T(8,128)} slice(f32[1024,512]{1,0:T(8,128)} %get-tuple-element.60), slice={[0:1023:2], [0:512:1]} | slice | bytes 2097152 | tf_op jit(solution)/shard_map/slice | solution.py:93
  204.0 6.3 %slice.383 = f32[511,512]{1,0:T(8,128)} slice(f32[1024,512]{1,0:T(8,128)} %get-tuple-element.60), slice={[2:1024:2], [0:512:1]} | slice | bytes 2093056 | tf_op jit(solution)/shard_map/slice | solution.py:93
  210.3 6.4 %slice.456 = f32[511,512]{1,0:T(8,128)} slice(f32[1024,512]{1,0:T(8,128)} %get-tuple-element.59), slice={[2:1024:2], [0:512:1]} | slice | bytes 2093056 | tf_op jit(solution)/shard_map/slice | solution.py:93
  236.2 4.7 %pad.139 = f32[512,512]{1,0:T(8,128)} pad(f32[256,512]{1,0:T(8,128)} %add.337, f32[]{:T(128)} %constant.71.clone.1), padding=1_0_1x0_0_0 | pad | bytes 1572868 | tf_op jit(solution)/shard_map/pad | solution.py:93
  243.3 8.6 %pad.141 = f32[1024,512]{1,0:T(8,128)} pad(f32[512,512]{1,0:T(8,128)} %add.339, f32[]{:T(128)} %constant.71.clone.1), padding=1_0_1x0_0_0 | pad | bytes 3145732 | tf_op jit(solution)/shard_map/pad | solution.py:93
  253.8 4.6 %pad.158 = f32[512,512]{1,0:T(8,128)} pad(f32[256,512]{1,0:T(8,128)} %pad_maximum_fusion.3, f32[]{:T(128)} %constant.71.clone.1), padding=0_1_1x0_0_0 | pad | bytes 1572868 | tf_op jit(solution)/shard_map/pad | solution.py:93
  258.4 4.6 %pad.159 = f32[512,512]{1,0:T(8,128)} pad(f32[256,512]{1,0:T(8,128)} %add.349, f32[]{:T(128)} %constant.71.clone.1), padding=1_0_1x0_0_0 | pad | bytes 1572868 | tf_op jit(solution)/shard_map/pad | solution.py:93
  270.3 8.8 %pad.140 = f32[1024,512]{1,0:T(8,128)} pad(f32[512,512]{1,0:T(8,128)} %pad_maximum_fusion, f32[]{:T(128)} %constant.71.clone.1), padding=0_1_1x0_0_0 | pad | bytes 3145732 | tf_op jit(solution)/shard_map/pad | solution.py:93
  279.1 4.8 %pad.161 = f32[1024,512]{1,0:T(8,128)} pad(f32[512,512]{1,0:T(8,128)S(1)} %copy-done.6, f32[]{:T(128)} %constant.71.clone.1), padding=1_0_1x0_0_0 | pad | bytes 3145732 | tf_op jit(solution)/shard_map/pad | solution.py:93
  285.2 4.8 %pad.160 = f32[1024,512]{1,0:T(8,128)} pad(f32[512,512]{1,0:T(8,128)S(1)} %pad_maximum_fusion.1, f32[]{:T(128)} %constant.71.clone.1), padding=0_1_1x0_0_0 | pad | bytes 3145732 | tf_op jit(solution)/shard_map/pad | solution.py:93
  290.8 34.3 %all-gather.4 = f32[8,1,512]{2,1,0:T(1,128)S(1)} all-gather(f32[1,1,512]{2,1,0:T(1,128)S(1)} %add_bitcast_fusion), channel_id=1, replica_groups=mesh['ep'=8,'tp'=4] {'ep'}, dimensions={0}, use_global_device_ids=true | all-gather | bytes 18432 | tf_op jit(solution)/shard_map/all_gather | solution.py:18
  325.8 26.1 %all-gather.3 = f32[8,1,512]{2,1,0:T(1,128)S(1)} all-gather(f32[1,1,512]{2,1,0:T(1,128)S(1)} %add_bitcast_fusion.1), channel_id=1, replica_groups=mesh['ep'=8,'tp'=4] {'ep'}, dimensions={0}, use_global_device_ids=true | all-gather | bytes 18432 | tf_op jit(solution)/shard_map/all_gather | solution.py:18
  352.0 12.4 %convolution_convert_fusion = bf16[1024,2048]{1,0:T(8,128)(2,1)} fusion(bf16[512,2048]{1,0:T(8,128)(2,1)S(1)} %copy-done, f32[1024,512]{1,0:T(8,128)} %pad.160, f32[1024,512]{1,0:T(8,128)} %pad.161, f32[1024,512]{1,0:T(8,128)} %pad.140, f32[1024,512]{1,0:T(8,128)} %pad.141, bf16[1024,2048]{1,0:T(8,128)(2,1)} %all-gather.10.cloned.1.call-done, ...), kind=kOutput, calls=%fused_computation.8 | convolution fusion | flops 4305453056 | bytes 20973568 | tf_op jit(solution)/shard_map/dot_general | solution.py:101
  364.4 6.5 %fusion.2 = f32[512,1024]{1,0:T(8,128)} fusion(bf16[512,2048]{1,0:T(8,128)(2,1)} %bitcast.16, bf16[1,2048,1024]{2,1,0:T(8,128)(2,1)} %all-gather.12.cloned.1.call-done), kind=kOutput, calls=%fused_computation.5 | convolution fusion | flops 2147483648 | bytes 8388608 | tf_op jit(solution)/shard_map/dot_general | solution.py:144
  370.9 6.3 %multiply_convert_fusion = bf16[512,1024]{1,0:T(8,128)(2,1)S(1)} fusion(f32[512,1024]{1,0:T(8,128)} %fusion.2, bf16[512,2048]{1,0:T(8,128)(2,1)} %bitcast.16, bf16[1,2048,1024]{2,1,0:T(8,128)(2,1)} %all-gather.14.cloned.1.call-done), kind=kOutput, calls=%fused_computation.50 | convolution fusion | flops 2150629376 | bytes 9437184 | tf_op jit(solution)/shard_map/dot_general | solution.py:145
  386.1 4.5 %all-to-all-start.1 = ((bf16[8,64,2048]{2,1,0:T(8,128)(2,1)}), bf16[8,64,2048]{2,1,0:T(8,128)(2,1)}, u32[]{:S(2)}, u32[]{:S(2)}) async-start(bf16[8,64,2048]{2,1,0:T(8,128)(2,1)} %bitcast.75), calls=%async_computation.2 | async-start | bytes 4194304 | tf_op jit(solution)/shard_map/all_to_all | solution.py:160
  390.9 38.8 %all-to-all-done.1 = bf16[8,64,2048]{2,1,0:T(8,128)(2,1)} async-done(((bf16[8,64,2048]{2,1,0:T(8,128)(2,1)}), bf16[8,64,2048]{2,1,0:T(8,128)(2,1)}, u32[]{:S(2)}, u32[]{:S(2)}) %all-to-all-start.1) | async-done | bytes 2097184 | tf_op jit(solution)/shard_map/all_to_all | solution.py:160
  (317 shorter events, 177.4 us)
Async XLA Ops:
  7.2 344.8 %copy-start = (bf16[512,2048]{1,0:T(8,128)(2,1)S(1)}, bf16[512,2048]{1,0:T(8,128)(2,1)}, u32[]{:S(2)}) copy-start(bf16[512,2048]{1,0:T(8,128)(2,1)} %param.28) | copy-start | bytes 6291460
  7.2 42.3 %all-gather.10.cloned.1.call-start = ((), (), s32[]{:S(2)}) async-start(), calls=%async_computation.3 | async-start | bytes 5242880 | tf_op jit(solution)/shard_map/all_gather | solution.py:60
  12.1 352.3 %all-gather.12.cloned.1.call-start = ((), (), s32[]{:S(2)}) async-start(), calls=%async_computation.5 | async-start | bytes 5242880 | tf_op jit(solution)/shard_map/all_gather | solution.py:139
  12.9 358.1 %all-gather.14.cloned.1.call-start = ((), (), s32[]{:S(2)}) async-start(), calls=%async_computation.6 | async-start | bytes 5242880 | tf_op jit(solution)/shard_map/all_gather | solution.py:140
  17.9 346.4 %all-to-all-start = ((bf16[8,64,2048]{2,1,0:T(8,128)(2,1)}), bf16[8,64,2048]{2,1,0:T(8,128)(2,1)}, u32[]{:S(2)}, u32[]{:S(2)}) async-start(bf16[8,64,2048]{2,1,0:T(8,128)(2,1)} %bitcast.76), calls=%async_computation.1 | async-start | bytes 4194304 | tf_op jit(solution)/shard_map/all_to_all | solution.py:134
  25.4 351.9 %all-gather.16.cloned.1.call-start = ((), (), s32[]{:S(2)}) async-start(), calls=%async_computation.7 | async-start | bytes 5242880 | tf_op jit(solution)/shard_map/all_gather | solution.py:141
  26.0 407.2 %reduce-scatter.2.cloned.1.call-start = ((), (), s32[]{:S(2)}) async-start(), calls=%async_computation.4 | async-start | bytes 5242880 | tf_op jit(solution)/shard_map/reduce_scatter | solution.py:100
  55.6 7.6 %collective-permute-start = (bf16[3,512]{1,0:T(4,128)(2,1)S(1)}, bf16[3,512]{1,0:T(4,128)(2,1)S(1)}, u32[]{:S(2)}, u32[]{:S(2)}) collective-permute-start(bf16[3,512]{1,0:T(4,128)(2,1)S(1)} %slice.497), channel_id=1, source_target_pairs={{0,4},{4,8},{8,12},{12,16},{16,20},{20,24},{24,28},{1,5},{5,9},{9,... | collective-permute-start | bytes 9224 | tf_op jit(solution)/shard_map/ppermute | solution.py:13
  203.8 15.5 %copy-start.26 = (f32[2,512]{1,0:T(2,128)S(1)}, f32[2,512]{1,0:T(2,128)}, u32[]{:S(2)}) copy-start(f32[2,512]{1,0:T(2,128)} %get-tuple-element.115) | copy-start | bytes 12292
  203.8 15.5 %copy-start.25 = (f32[2,512]{1,0:T(2,128)S(1)}, f32[2,512]{1,0:T(2,128)}, u32[]{:S(2)}) copy-start(f32[2,512]{1,0:T(2,128)} %get-tuple-element.114) | copy-start | bytes 12292
  203.8 15.5 %copy-start.45 = (f32[1,512]{1,0:T(1,128)S(1)}, f32[1,512]{1,0:T(1,128)}, u32[]{:S(2)}) copy-start(f32[1,512]{1,0:T(1,128)} %get-tuple-element.91) | copy-start | bytes 6148
  203.8 15.5 %copy-start.46 = (f32[1,512]{1,0:T(1,128)S(1)}, f32[1,512]{1,0:T(1,128)}, u32[]{:S(2)}) copy-start(f32[1,512]{1,0:T(1,128)} %get-tuple-element.92) | copy-start | bytes 6148
  203.9 15.5 %copy-start.47 = (f32[1,512]{1,0:T(1,128)S(1)}, f32[1,512]{1,0:T(1,128)}, u32[]{:S(2)}) copy-start(f32[1,512]{1,0:T(1,128)} %get-tuple-element.93) | copy-start | bytes 6148
  203.9 15.5 %copy-start.48 = (f32[1,512]{1,0:T(1,128)S(1)}, f32[1,512]{1,0:T(1,128)}, u32[]{:S(2)}) copy-start(f32[1,512]{1,0:T(1,128)} %get-tuple-element.94) | copy-start | bytes 6148
  203.9 15.6 %copy-start.22 = (f32[3,512]{1,0:T(4,128)S(1)}, f32[3,512]{1,0:T(4,128)}, u32[]{:S(2)}) copy-start(f32[3,512]{1,0:T(4,128)} %slice.425) | copy-start | bytes 18436
  203.9 15.6 %copy-start.23 = (f32[3,512]{1,0:T(4,128)S(1)}, f32[3,512]{1,0:T(4,128)}, u32[]{:S(2)}) copy-start(f32[3,512]{1,0:T(4,128)} %slice.442) | copy-start | bytes 18436
  203.9 15.6 %copy-start.44 = (f32[1,512]{1,0:T(1,128)S(1)}, f32[1,512]{1,0:T(1,128)}, u32[]{:S(2)}) copy-start(f32[1,512]{1,0:T(1,128)} %slice.546) | copy-start | bytes 6148
  203.9 15.7 %copy-start.43 = (f32[1,512]{1,0:T(1,128)S(1)}, f32[1,512]{1,0:T(1,128)}, u32[]{:S(2)}) copy-start(f32[1,512]{1,0:T(1,128)} %slice.514) | copy-start | bytes 6148
  203.9 15.7 %copy-start.21 = (f32[7,512]{1,0:T(8,128)S(1)}, f32[7,512]{1,0:T(8,128)}, u32[]{:S(2)}) copy-start(f32[7,512]{1,0:T(8,128)} %slice.444) | copy-start | bytes 43012
  203.9 15.8 %copy-start.42 = (f32[1,512]{1,0:T(1,128)S(1)}, f32[1,512]{1,0:T(1,128)}, u32[]{:S(2)}) copy-start(f32[1,512]{1,0:T(1,128)} %slice.545) | copy-start | bytes 6148
  203.9 15.8 %copy-start.41 = (f32[1,512]{1,0:T(1,128)S(1)}, f32[1,512]{1,0:T(1,128)}, u32[]{:S(2)}) copy-start(f32[1,512]{1,0:T(1,128)} %slice.513) | copy-start | bytes 6148
  203.9 15.9 %copy-start.17 = (f32[15,512]{1,0:T(8,128)S(1)}, f32[15,512]{1,0:T(8,128)}, u32[]{:S(2)}) copy-start(f32[15,512]{1,0:T(8,128)} %slice.413) | copy-start | bytes 92164
  204.0 15.9 %copy-start.18 = (f32[15,512]{1,0:T(8,128)S(1)}, f32[15,512]{1,0:T(8,128)}, u32[]{:S(2)}) copy-start(f32[15,512]{1,0:T(8,128)} %slice.446) | copy-start | bytes 92164
  386.1 43.6 %all-to-all-start.1 = ((bf16[8,64,2048]{2,1,0:T(8,128)(2,1)}), bf16[8,64,2048]{2,1,0:T(8,128)(2,1)}, u32[]{:S(2)}, u32[]{:S(2)}) async-start(bf16[8,64,2048]{2,1,0:T(8,128)(2,1)} %bitcast.75), calls=%async_computation.2 | async-start | bytes 4194304 | tf_op jit(solution)/shard_map/all_to_all | solution.py:160
  (39 other events, 172.5 us)
Sparse Core Ops, SparseCore 0:
  12.2 37.1 all-gather.9
  51.0 34.9 all-gather.11
  87.6 34.9 all-gather.13
  124.0 34.4 all-gather.15
  364.5 41.9 reduce-scatter.1
where the time goes:
time: 445 us; the launch traced here: 440 us
  local copies, waits for them, and re-layouts  183 us (41%)
  waiting for transfers between devices  62.8 us (14%)
  blocking collectives  60.4 us (14%)
  other arithmetic  54.9 us (12%)
  matrix products  48.2 us (11%)
  starting transfers between devices  15.7 us (4%)
  between operations  14.9 us (3%)
    slice x68, local copies, waits for them, and re-layouts, run_mixer(): lax.associative_scan(chain_link, (jnp.exp(log_decay), drive), axis=0)  128 us
    all_gather x2, blocking collectives, entering(): gathered = jax.tree.map(lambda a: lax.all_gather(a, axis), part)  60.4 us
    pad x36, local copies, waits for them, and re-layouts, run_mixer(): lax.associative_scan(chain_link, (jnp.exp(log_decay), drive), axis=0)  47.7 us
    all_to_all x1, waiting for transfers between devices, run_experts(): lax.all_to_all(expert_done, 'ep', split_axis=0, concat_axis=0, tiled=True)  38.8 us
    add x17, other arithmetic, chain_link(): return (later[0] * earlier[0], later[0] * earlier[1] + later[1])  23.1 us
    all_gather x1, waiting for transfers between devices, run_mixer(): piece = lax.all_gather(mixer_in, 'tp', axis=0, tiled=True)  22.1 us
    dot_general x1, matrix products, run_mixer(): jnp.dot(mixed, w_mix_out, preferred_element_type=jnp.float32)  12.4 us
    add x17, other arithmetic, run_mixer(): lax.associative_scan(chain_link, (jnp.exp(log_decay), drive), axis=0)  9.91 us
  transfers between devices with their start and end apart: 8, of which 2 were waited for; matrix products, arithmetic and copies ran while one was open for 63% of the time, Pallas kernels for 0%

commit v1 on v0

--- a/solution.py
+++ b/solution.py
@@ -1,29 +1,14 @@
+import functools
+
 import jax
 import jax.numpy as jnp
 from jax import lax
+from jax.experimental import pallas as pl
+from jax.experimental.pallas import tpu as pltpu
 from jax.sharding import PartitionSpec as P
 
 epsilon = 1e-06
 gate_const = 8.0
-
-
-def from_behind(block, axis, distance):
-    devices = range(lax.axis_size(axis))
-    route = [(i - distance, i) for i in devices if i - distance in devices]
-    return lax.ppermute(block, axis, route)
-
-
-def entering(part, axis, combine, identity):
-    place = lax.axis_index(axis)
-    gathered = jax.tree.map(lambda a: lax.all_gather(a, axis), part)
-    state = jax.tree.map(lambda a, e: jnp.zeros_like(a) + jnp.asarray(e, a.dtype), part, identity)
-
-    def one(step, state):
-        return combine(
-            state, jax.tree.map(lambda a: lax.dynamic_index_in_dim(a, step, 0, False), gathered)
-        )
-
-    return lax.fori_loop(0, place, one, state)
 
 
 def norm_rows(values, gain_vec):
@@ -32,15 +17,186 @@
     return (value_f32 * inv_scale * gain_vec.astype(jnp.float32)).astype(jnp.bfloat16)
 
 
-def chain_link(earlier, later):
-    return (later[0] * earlier[0], later[0] * earlier[1] + later[1])
-
-
-def block_diagonal(head_maps):
+MESH = pl.DeviceIdType.MESH
+LANES = 128
+SEGMENTS = 8
+EDGE = 16
+
+
+def chunk_gates(rows, chunk, prev, x_ref, maps_ref, taps_ref, slow_ref, kick_ref, a_s, b_s):
+    start = pl.multiple_of(chunk * rows, rows)
+    here = x_ref[pl.ds(start, rows), :].astype(jnp.float32)
+    kick = kick_ref[pl.ds(start, rows), :]
+    taps = taps_ref[...]
+    tap_count = taps.shape[0]
+    groups = maps_ref.shape[0]
+    per = kick.shape[1] // groups
+    dim = LANES // per
+    lane = lax.broadcasted_iota(jnp.int32, (rows, LANES), 1)
+    for g in range(groups):
+        cols = slice(g * LANES, (g + 1) * LANES)
+        x = here[:, cols]
+        window = jnp.concatenate([prev[:, cols], x], axis=0)
+        conv = taps[tap_count - 1 : tap_count, cols] * x
+        for k in range(tap_count - 1):
+            conv = conv + taps[k : k + 1, cols] * pltpu.roll(window, tap_count - 1 - k, 0)[EDGE:]
+        pre = jnp.dot(
+            conv.astype(jnp.bfloat16), maps_ref[g], preferred_element_type=jnp.float32
+        )
+        recur = jax.nn.sigmoid(pre[:, :LANES])
+        inject = jax.nn.sigmoid(pre[:, LANES:])
+        wide = kick[:, g * per : g * per + 1]
+        for j in range(1, per):
+            wide = jnp.where(lane >= j * dim, kick[:, g * per + j : g * per + j + 1], wide)
+        log_decay = -gate_const * recur * slow_ref[:, cols] + wide
+        decay = jnp.exp(log_decay)
+        twice = 2.0 * log_decay
+        series = 1.0 + twice * (1.0 / 8.0)
+        for m in (7.0, 6.0, 5.0, 4.0, 3.0, 2.0):
+            series = 1.0 + twice * (1.0 / m) * series
+        lost = jnp.where(twice > -0.5, -twice * series, 1.0 - decay * decay)
+        a_s[g, pl.ds(start, rows), :] = decay
+        b_s[g, pl.ds(start, rows), :] = jnp.sqrt(lost) * inject * conv
+
+
+def mixer_kernel(
+    n,
+    x_ref,
+    gate_ref,
+    maps_ref,
+    taps_ref,
+    slow_ref,
+    kick_ref,
+    out_ref,
+    a_s,
+    b_s,
+    gelu_s,
+    enter_s,
+    halo_s,
+    own_s,
+    ends_s,
+    halo_send,
+    halo_recv,
+    end_send,
+    end_recv,
+):
+    me = lax.axis_index("ep")
+    total = x_ref.shape[0]
+    rows = total // SEGMENTS
+    groups = maps_ref.shape[0]
+    barrier = pltpu.get_barrier_semaphore()
+
+    @pl.loop(1, n)
+    def _(d):
+        pl.semaphore_signal(
+            barrier, inc=1, device_id={"ep": lax.rem(me + d, n)}, device_id_type=MESH
+        )
+
+    def later_chunk(chunk):
+        ahead = pl.multiple_of(chunk * rows - EDGE, EDGE)
+        prev = x_ref[pl.ds(ahead, EDGE), :].astype(jnp.float32)
+        chunk_gates(rows, chunk, prev, x_ref, maps_ref, taps_ref, slow_ref, kick_ref, a_s, b_s)
+
+    pl.loop(1, 2)(later_chunk)
+    pl.semaphore_wait(barrier, n - 1)
+    halo = pltpu.make_async_remote_copy(
+        src_ref=x_ref.at[pl.ds(total - EDGE, EDGE), :],
+        dst_ref=halo_s,
+        send_sem=halo_send,
+        recv_sem=halo_recv,
+        device_id={"ep": lax.rem(me + 1, n)},
+        device_id_type=MESH,
+    )
+    halo.start()
+    pl.loop(2, SEGMENTS)(later_chunk)
+    halo.wait()
+    prev = jnp.where(me > 0, halo_s[...].astype(jnp.float32), 0.0)
+    chunk_gates(rows, 0, prev, x_ref, maps_ref, taps_ref, slow_ref, kick_ref, a_s, b_s)
+
+    ones = jnp.ones((SEGMENTS, LANES), jnp.float32)
+    zeros = jnp.zeros((SEGMENTS, LANES), jnp.float32)
+
+    def one(step, carry):
+        after = []
+        for g in range(groups):
+            prod, state = carry[g]
+            at = pl.ds(step, SEGMENTS, stride=rows)
+            decay = a_s[g, at, :]
+            state = decay * state + b_s[g, at, :]
+            prod = decay * prod
+            a_s[g, at, :] = prod
+            b_s[g, at, :] = state
+            after.append((prod, state))
+        return tuple(after)
+
+    ends = lax.fori_loop(0, rows, one, tuple((ones, zeros) for _ in range(groups)), unroll=4)
+
+    for g in range(groups):
+        prod, state = ends[g]
+        p, h = ones[:1], zeros[:1]
+        for s in range(SEGMENTS):
+            enter_s[0, g, s : s + 1, :] = p
+            enter_s[1, g, s : s + 1, :] = h
+            h = prod[s : s + 1] * h + state[s : s + 1]
+            p = prod[s : s + 1] * p
+        own_s[0:1, g * LANES : (g + 1) * LANES] = p
+        own_s[1:2, g * LANES : (g + 1) * LANES] = h
+    own_s[2:, :] = jnp.zeros_like(own_s[2:, :])
+    ends_s[me] = own_s[...]
+
+    def end_copy(sender, target):
+        return pltpu.make_async_remote_copy(
+            src_ref=own_s,
+            dst_ref=ends_s.at[sender],
+            send_sem=end_send.at[target],
+            recv_sem=end_recv.at[sender],
+            device_id={"ep": target},
+            device_id_type=MESH,
+        )
+
+    @pl.loop(1, n)
+    def _(d):
+        end_copy(me, lax.rem(me + d, n)).start()
+
+    @pl.loop(0, SEGMENTS)
+    def _(c):
+        at = pl.ds(pl.multiple_of(c * rows, rows), rows)
+        for g in range(groups):
+            gate = gate_ref[at, g * LANES : (g + 1) * LANES].astype(jnp.float32)
+            gelu_s[g, at, :] = jax.nn.gelu(gate)
+
+    @pl.loop(1, n)
+    def _(d):
+        end_copy(me, lax.rem(me + d, n)).wait_send()
+
+    @pl.loop(1, n)
+    def _(d):
+        end_copy(lax.rem(me + d, n), lax.rem(me + d, n)).wait_recv()
+
+    def fold(s, carried):
+        pair = ends_s[s]
+        return jnp.where(s < me, pair[0:1] * carried + pair[1:2], carried)
+
+    carried = lax.fori_loop(0, n, fold, jnp.zeros((1, groups * LANES), jnp.float32))
+    for g in range(groups):
+        enter_s[1, g] = enter_s[0, g] * carried[:, g * LANES : (g + 1) * LANES] + enter_s[1, g]
+
+    @pl.loop(0, SEGMENTS)
+    def _(c):
+        at = pl.ds(pl.multiple_of(c * rows, rows), rows)
+        for g in range(groups):
+            state = b_s[g, at, :] + a_s[g, at, :] * enter_s[1, g, pl.ds(c, 1), :]
+            out_ref[at, g * LANES : (g + 1) * LANES] = (state * gelu_s[g, at, :]).astype(
+                out_ref.dtype
+            )
+
+
+def paired_maps(head_maps):
     head_count, head_dim, _ = head_maps.shape
-    head_eye = jnp.eye(head_count, dtype=head_maps.dtype)
-    spread = head_maps[:, :, None, :] * head_eye[:, None, :, None]
-    return spread.reshape(head_count * head_dim, head_count * head_dim)
+    per = LANES // head_dim
+    grouped = head_maps.reshape(head_count // per, per, head_dim, 1, head_dim)
+    eye = jnp.eye(per, dtype=head_maps.dtype)[None, :, None, :, None]
+    return (grouped * eye).reshape(head_count // per, LANES, LANES)
 
 
 def run_mixer(
@@ -56,47 +212,44 @@
     w_mix_out,
 ):
     mixer_in = norm_rows(mix_tokens, mix_gain)
-    col_count = w_branch.shape[1]
     piece = lax.all_gather(mixer_in, "tp", axis=0, tiled=True)
-    first = jnp.dot(piece, w_branch, preferred_element_type=jnp.float32).astype(jnp.bfloat16)
-    second = jnp.dot(piece, w_gate_branch, preferred_element_type=jnp.float32).astype(jnp.bfloat16)
-    both_proj = jnp.stack([first, second], axis=0)
-    branch_x = both_proj[0]
-    branch_gate = both_proj[1]
-    row_count = branch_x.shape[0]
-    tap_count = conv_taps.shape[0]
-    rim_rows = from_behind(branch_x[row_count - (tap_count - 1) :], "ep", 1)
-    extended = jnp.concatenate([rim_rows, branch_x], axis=0).astype(jnp.float32)
-    tap_values = conv_taps.astype(jnp.float32)
-    conv_out = tap_values[tap_count - 1] * extended[tap_count - 1 :]
-    for index_value in range(tap_count - 1):
-        conv_out = (
-            conv_out + tap_values[index_value] * extended[index_value : index_value + row_count]
-        )
-    conv_low = conv_out.astype(jnp.bfloat16)
-    head_count = recur_gate_w.shape[0]
-    head_dim = recur_gate_w.shape[1]
-    gate_maps = jnp.concatenate(
-        [block_diagonal(recur_gate_w), block_diagonal(inject_gate_w)], axis=1
-    )
-    gate_pre = jnp.dot(conv_low, gate_maps, preferred_element_type=jnp.float32)
-    recur = jax.nn.sigmoid(gate_pre[:, :col_count])
-    inject = jax.nn.sigmoid(gate_pre[:, col_count:])
-    slowness = jax.nn.softplus(-decay_logit)
-    widen = (
-        jnp.arange(col_count, dtype=jnp.int32)[None, :] // head_dim
-        == jnp.arange(head_count, dtype=jnp.int32)[:, None]
-    ).astype(jnp.float32)
-    kick_wide = jnp.dot(decay_kick, widen, precision=lax.Precision.HIGHEST)
-    log_decay = -gate_const * recur * slowness[None, :] + kick_wide
-    drive = jnp.sqrt(-jnp.expm1(2.0 * log_decay)) * inject * conv_out
-    acc_decay, local_state = lax.associative_scan(chain_link, (jnp.exp(log_decay), drive), axis=0)
-    identity = (jnp.ones((col_count,), jnp.float32), jnp.zeros((col_count,), jnp.float32))
-    carried = entering(
-        (acc_decay[row_count - 1], local_state[row_count - 1]), "ep", chain_link, identity
-    )
-    state = local_state + acc_decay * carried[1][None, :]
-    mixed = (state * jax.nn.gelu(branch_gate.astype(jnp.float32))).astype(jnp.bfloat16)
+    branch_x = jnp.dot(piece, w_branch, preferred_element_type=jnp.float32).astype(jnp.bfloat16)
+    branch_gate = jnp.dot(piece, w_gate_branch, preferred_element_type=jnp.float32).astype(
+        jnp.bfloat16
+    )
+    maps = jnp.concatenate([paired_maps(recur_gate_w), paired_maps(inject_gate_w)], axis=2)
+    slowness = jax.nn.softplus(-decay_logit)[None, :]
+    n = lax.axis_size("ep")
+    row_count, col_count = branch_x.shape
+    groups = col_count // LANES
+    plane = pltpu.VMEM((groups, row_count, LANES), jnp.float32)
+    mixed = pl.pallas_call(
+        functools.partial(mixer_kernel, n),
+        out_shape=jax.ShapeDtypeStruct((row_count, col_count), jnp.bfloat16),
+        in_specs=[pl.BlockSpec(memory_space=pltpu.VMEM)] * 6,
+        out_specs=pl.BlockSpec(memory_space=pltpu.VMEM),
+        scratch_shapes=[
+            plane,
+            plane,
+            plane,
+            pltpu.VMEM((2, groups, SEGMENTS, LANES), jnp.float32),
+            pltpu.VMEM((EDGE, col_count), jnp.bfloat16),
+            pltpu.VMEM((8, col_count), jnp.float32),
+            pltpu.VMEM((n, 8, col_count), jnp.float32),
+            pltpu.SemaphoreType.DMA,
+            pltpu.SemaphoreType.DMA,
+            pltpu.SemaphoreType.DMA((n,)),
+            pltpu.SemaphoreType.DMA((n,)),
+        ],
+        compiler_params=pltpu.CompilerParams(
+            collective_id=0, has_side_effects=True, vmem_limit_bytes=24 * 1024 * 1024
+        ),
+        cost_estimate=pl.CostEstimate(
+            flops=100 * row_count * col_count,
+            bytes_accessed=40 * row_count * col_count,
+            transcendentals=6 * row_count * col_count,
+        ),
+    )(branch_x, branch_gate, maps, conv_taps.astype(jnp.float32), slowness, decay_kick)
     return lax.psum_scatter(
         jnp.dot(mixed, w_mix_out, preferred_element_type=jnp.float32).astype(jnp.bfloat16),
         "tp",

time: 445 us -> 232 us (0.52); the launches traced: 440 us -> 232 us
  local copies, waits for them, and re-layouts: 183 us -> 1.84 us
  waiting for transfers between devices: 62.8 us -> 129 us
  blocking collectives: 60.4 us -> 0 us
  other arithmetic: 54.9 us -> 9.03 us
  Pallas kernels: 0 us -> 28.6 us
  matrix products: 48.2 us -> 35.6 us
    slice x71 -> x1, local copies, waits for them, and re-layouts: 128 us -> 0.22 us  [the longest x68 128 us: run_mixer(): lax.associative_scan(chain_link, (jnp.exp(log_decay), drive), axis=0)]
    all_gather x2 -> x0, blocking collectives: 60.4 us -> none  [entering(): gathered = jax.tree.map(lambda a: lax.all_gather(a, axis), part)]
    pad x36 -> x0, local copies, waits for them, and re-layouts: 47.7 us -> none  [run_mixer(): lax.associative_scan(chain_link, (jnp.exp(log_decay), drive), axis=0)]
    add x35 -> x0, other arithmetic: 33.9 us -> none  [the longest x17 23.1 us: chain_link(): return (later[0] * earlier[0], later[0] * earlier[1] + later[1])]
    all_gather x1, waiting for transfers between devices: 0.02 us -> 30 us  [run_experts(): lax.all_gather(down_mat, 'tp', axis=0, tiled=True)]
    pallas_call x0 -> x1, Pallas kernels: none -> 28.6 us  [run_mixer(): pl.pallas_call(functools.partial(mixer_kernel, n), out_shape=jax.ShapeDty...]
    all_gather x1, waiting for transfers between devices: 0.01 us -> 26 us  [run_experts(): lax.all_gather(up_mat, 'tp', axis=1, tiled=True)]
    all_to_all x1, waiting for transfers between devices: 38.8 us -> 48.5 us  [run_experts(): lax.all_to_all(expert_done, 'ep', split_axis=0, concat_axis=0, tiled=True)]
  transfers between devices with their start and end apart: 8 -> 7, of which waited for: 2 -> 4; matrix products, arithmetic and copies ran while one was open for 63% -> 18% of each run, Pallas kernels for 0% -> 12%
where the time goes in v1:
time: 232 us
  waiting for transfers between devices  129 us (56%)
  matrix products  35.6 us (15%)
  Pallas kernels  28.6 us (12%)
  between operations  14.1 us (6%)
  starting transfers between devices  13.3 us (6%)
  other arithmetic  9.03 us (4%)
    all_to_all x1, waiting for transfers between devices, run_experts(): lax.all_to_all(expert_done, 'ep', split_axis=0, concat_axis=0, tiled=True)  48.5 us
    all_gather x1, waiting for transfers between devices, run_experts(): lax.all_gather(down_mat, 'tp', axis=0, tiled=True)  30 us
    pallas_call x1, Pallas kernels, run_mixer(): pl.pallas_call(functools.partial(mixer_kernel, n), out_shape=jax.ShapeDty...  28.6 us
    all_gather x1, waiting for transfers between devices, run_experts(): lax.all_gather(up_mat, 'tp', axis=1, tiled=True)  26 us
    all_gather x1, waiting for transfers between devices, run_mixer(): piece = lax.all_gather(mixer_in, 'tp', axis=0, tiled=True)  22.7 us
    all_to_all x1, starting transfers between devices, run_experts(): lax.all_to_all(outgoing, 'ep', split_axis=0, concat_axis=0, tiled=True)  7.44 us
    dot_general x1, matrix products, run_experts(): jnp.dot(arrived, full_gate, preferred_element_type=jnp.float32)  6.47 us
    dot_general x1, matrix products, run_experts(): jnp.dot(arrived, full_up, preferred_element_type=jnp.float32)  5.91 us
  transfers between devices with their start and end apart: 7, of which 4 were waited for; matrix products, arithmetic and copies ran while one was open for 18% of the time, Pallas kernels for 12%

profile of v1, /device:TPU:0, one launch (start us, length us, event | category | flops | bytes accessed | tf_op | source)
XLA Modules:
  0.0 231.6 jit_solution(3152801715540026271)
XLA Ops:
  7.2 0.8 convert_element_type.92
  8.1 1.5 fusion.4
  9.6 2.5 %fusion.6 = bf16[256,2048]{1,0:T(8,128)(2,1)} fusion(bf16[256,2048]{1,0:T(8,128)(2,1)} %param.17, f32[2048]{0:T(1024)S(1)} %convert_element_type.92, f32[256]{0:T(256)S(1)} %add_rsqrt_fusion), kind=kLoop, calls=%fused_computation.16 | loop fusion | flops 2097152 | bytes 2106368 | tf_op jit(solution)/shard_map/convert_element_type | solution.py:17
  12.2 0.7 all-gather.10.cloned.1.call-update
  12.9 0.7 all-gather.12.cloned.1.call-update
  15.7 2.4 %convolution_convert_fusion.5 = bf16[512,2048]{1,0:T(8,128)(2,1)} fusion(bf16[128,2048]{1,0:T(8,128)(2,1)S(1)} %copy-done.2, f32[2048]{0:T(1024)S(1)} %convert_element_type.103, f32[128]{0:T(128)S(1)} %add_rsqrt_fusion.1, s32[256]{0:T(256)S(1)} %get-tuple-element.9, s32[256]{0:T(256)S(1)} %get-tuple-element.8), kind=kOutput, calls=%fused_computation.10 | convolution fusion | flops 304316416 | bytes 2632192 | tf_op jit(solution)/shard_map/dot_general | solution.py:284
  18.1 7.4 %all-to-all-start = ((bf16[8,64,2048]{2,1,0:T(8,128)(2,1)}), bf16[8,64,2048]{2,1,0:T(8,128)(2,1)}, u32[]{:S(2)}, u32[]{:S(2)}) async-start(bf16[8,64,2048]{2,1,0:T(8,128)(2,1)} %bitcast.54), calls=%async_computation.1 | async-start | bytes 4194304 | tf_op jit(solution)/shard_map/all_to_all | solution.py:287
  26.8 22.7 %all-gather.8.cloned.1.call-done = bf16[1024,2048]{1,0:T(8,128)(2,1)} async-done(((bf16[256,2048]{1,0:T(8,128)(2,1)}), bf16[1024,2048]{1,0:T(8,128)(2,1)}) %all-gather.8.cloned.1.call-update) | async-done | bytes 4194320 | tf_op jit(solution)/shard_map/all_gather | solution.py:215
  49.4 5.3 %convolution_convert_fusion.7.gate_ref = bf16[1024,512]{1,0:T(8,128)(2,1)S(1)} fusion(bf16[1024,2048]{1,0:T(8,128)(2,1)} %all-gather.8.cloned.1.call-done, bf16[2048,512]{1,0:T(8,128)(2,1)} %param.20), kind=kOutput, calls=%fused_computation.18 | convolution fusion | flops 2148007936 | bytes 7340032 | tf_op jit(solution)/shard_map/dot_general | solution.py:217
  54.8 2.3 %convolution_convert_fusion.8.x_ref = bf16[1024,512]{1,0:T(8,128)(2,1)S(1)} fusion(bf16[1024,2048]{1,0:T(8,128)(2,1)S(1)} %copy-done.11, bf16[2048,512]{1,0:T(8,128)(2,1)S(1)} %copy-done.12), kind=kOutput, calls=%fused_computation.19 | convolution fusion | flops 2148007936 | bytes 7340032 | tf_op jit(solution)/shard_map/dot_general | solution.py:216
  57.1 28.6 %shard_map.176 = bf16[1024,512]{1,0:T(8,128)(2,1)S(1)} custom-call(bf16[1024,512]{1,0:T(8,128)(2,1)S(1)} %convolution_convert_fusion.8.x_ref, bf16[1024,512]{1,0:T(8,128)(2,1)S(1)} %convolution_convert_fusion.7.gate_ref, bf16[4,128,256]{2,1,0:T(8,128)(2,1)S(1)} %pad_maximum_fusion.maps_ref, f32[4,512]{1,0:T(4,128)S(1)} %convert_element_type.97.taps_ref, ...), custom_call_target="tpu_custom_call" | custom-call | flops 52428800 | bytes 20971520 | tf_op jit(solution)/shard_map/pallas_call | solution.py:226
  85.8 4.3 %convolution_convert_fusion = bf16[1024,2048]{1,0:T(8,128)(2,1)} fusion(bf16[1024,512]{1,0:T(8,128)(2,1)S(1)} %shard_map.176, bf16[512,2048]{1,0:T(8,128)(2,1)S(1)} %copy-done), kind=kOutput, calls=%fused_computation.5 | convolution fusion | flops 2149580800 | bytes 7340032 | tf_op jit(solution)/shard_map/dot_general | solution.py:254
  90.2 6.5 %fusion.2 = f32[512,1024]{1,0:T(8,128)} fusion(bf16[512,2048]{1,0:T(8,128)(2,1)} %bitcast.10, bf16[1,2048,1024]{2,1,0:T(8,128)(2,1)} %all-gather.10.cloned.1.call-done), kind=kOutput, calls=%fused_computation.2 | convolution fusion | flops 2147483648 | bytes 8388608 | tf_op jit(solution)/shard_map/dot_general | solution.py:297
  96.6 26.0 %all-gather.12.cloned.1.call-done = bf16[1,2048,1024]{2,1,0:T(8,128)(2,1)} async-done(((bf16[1,2048,256]{2,1,0:T(8,128)(2,1)}), bf16[1,2048,1024]{2,1,0:T(8,128)(2,1)}) %all-gather.12.cloned.1.call-update) | async-done | bytes 4194320 | tf_op jit(solution)/shard_map/all_gather | solution.py:293
  122.6 5.9 %multiply_convert_fusion = bf16[512,1024]{1,0:T(8,128)(2,1)S(1)} fusion(f32[512,1024]{1,0:T(8,128)} %fusion.2, bf16[512,2048]{1,0:T(8,128)(2,1)} %bitcast.10, bf16[1,2048,1024]{2,1,0:T(8,128)(2,1)} %all-gather.12.cloned.1.call-done), kind=kOutput, calls=%fused_computation.17 | convolution fusion | flops 2150629376 | bytes 9437184 | tf_op jit(solution)/shard_map/dot_general | solution.py:298
  128.5 30.0 %all-gather.14.cloned.1.call-done = bf16[1,1024,2048]{2,1,0:T(8,128)(2,1)} async-done(((bf16[1,256,2048]{2,1,0:T(8,128)(2,1)}), bf16[1,1024,2048]{2,1,0:T(8,128)(2,1)}) %all-gather.14.cloned.1.call-update) | async-done | bytes 4194320 | tf_op jit(solution)/shard_map/all_gather | solution.py:294
  158.5 2.1 convolution_convert_fusion.4
  160.6 2.0 convolution_convert_fusion.3
  162.6 0.7 convolution_convert_fusion.2
  163.3 0.7 convolution_convert_fusion.1
  164.0 3.2 %add_convert_fusion = bf16[512,2048]{1,0:T(8,128)(2,1)} fusion(bf16[512,2048]{1,0:T(8,128)(2,1)S(1)} %convolution_convert_fusion.1, bf16[512,2048]{1,0:T(8,128)(2,1)S(1)} %convolution_convert_fusion.2, bf16[512,2048]{1,0:T(8,128)(2,1)S(1)} %convolution_convert_fusion.3, bf16[512,2048]{1,0:T(8,128)(2,1)S(1)} %convolution_convert_fusion.4), kind=kLoop, calls=%fused_computation.4 | loop fusion | flops 8388608 | bytes 10485760 | tf_op jit(solution)/shard_map/convert_element_type | solution.py:312
  167.2 5.6 %all-to-all-start.1 = ((bf16[8,64,2048]{2,1,0:T(8,128)(2,1)}), bf16[8,64,2048]{2,1,0:T(8,128)(2,1)}, u32[]{:S(2)}, u32[]{:S(2)}) async-start(bf16[8,64,2048]{2,1,0:T(8,128)(2,1)} %bitcast.53), calls=%async_computation.2 | async-start | bytes 4194304 | tf_op jit(solution)/shard_map/all_to_all | solution.py:313
  173.1 48.5 %all-to-all-done.1 = bf16[8,64,2048]{2,1,0:T(8,128)(2,1)} async-done(((bf16[8,64,2048]{2,1,0:T(8,128)(2,1)}), bf16[8,64,2048]{2,1,0:T(8,128)(2,1)}, u32[]{:S(2)}, u32[]{:S(2)}) %all-to-all-start.1) | async-done | bytes 2097184 | tf_op jit(solution)/shard_map/all_to_all | solution.py:313
  221.6 3.4 %convolution_convert_fusion.6 = bf16[128,2048]{1,0:T(8,128)(2,1)} fusion(bf16[512,2048]{1,0:T(8,128)(2,1)} %bitcast.18, f32[128]{0:T(128)S(1)} %get-tuple-element.7, s32[128]{0:T(128)S(1)} %get-tuple-element.5, f32[128]{0:T(128)S(1)} %get-tuple-element.6, s32[128]{0:T(128)S(1)} %get-tuple-element.4), kind=kOutput, calls=%fused_computation.13 | convolution fusion | flops 1611202560 | bytes 2623488 | tf_op jit(solution)/shard_map/dot_general | solution.py:321
  (68 shorter events, 3.6 us)
Async XLA Ops:
  7.2 78.6 %copy-start = (bf16[512,2048]{1,0:T(8,128)(2,1)S(1)}, bf16[512,2048]{1,0:T(8,128)(2,1)}, u32[]{:S(2)}) copy-start(bf16[512,2048]{1,0:T(8,128)(2,1)} %param.26) | copy-start | bytes 6291460
  7.2 42.3 %all-gather.8.cloned.1.call-start = ((), (), s32[]{:S(2)}) async-start(), calls=%async_computation.3 | async-start | bytes 5242880 | tf_op jit(solution)/shard_map/all_gather | solution.py:215
  12.1 2.1 copy-start.6
  12.1 3.4 %copy-start.7 = (bf16[2048]{0:T(1024)(128)(2,1)S(1)}, bf16[2048]{0:T(1024)(128)(2,1)}, u32[]{:S(2)}) copy-start(bf16[2048]{0:T(1024)(128)(2,1)} %param.28) | copy-start | bytes 12292
  12.1 3.5 %copy-start.2 = (bf16[128,2048]{1,0:T(8,128)(2,1)S(1)}, bf16[128,2048]{1,0:T(8,128)(2,1)}, u32[]{:S(2)}) copy-start(bf16[128,2048]{1,0:T(8,128)(2,1)} %param.27) | copy-start | bytes 1572868
  12.1 78.1 %all-gather.10.cloned.1.call-start = ((), (), s32[]{:S(2)}) async-start(), calls=%async_computation.5 | async-start | bytes 5242880 | tf_op jit(solution)/shard_map/all_gather | solution.py:292
  12.9 109.8 %all-gather.12.cloned.1.call-start = ((), (), s32[]{:S(2)}) async-start(), calls=%async_computation.6 | async-start | bytes 5242880 | tf_op jit(solution)/shard_map/all_gather | solution.py:293
  13.6 144.9 %all-gather.14.cloned.1.call-start = ((), (), s32[]{:S(2)}) async-start(), calls=%async_computation.7 | async-start | bytes 5242880 | tf_op jit(solution)/shard_map/all_gather | solution.py:294
  18.1 7.5 %copy-start.3 = (bf16[8,64,64]{2,1,0:T(8,128)(2,1)S(1)}, bf16[8,64,64]{2,1,0:T(8,128)(2,1)}, u32[]{:S(2)}) copy-start(bf16[8,64,64]{2,1,0:T(8,128)(2,1)} %param.22) | copy-start | bytes 196612
  18.1 7.8 %copy-start.4 = (bf16[8,64,64]{2,1,0:T(8,128)(2,1)S(1)}, bf16[8,64,64]{2,1,0:T(8,128)(2,1)}, u32[]{:S(2)}) copy-start(bf16[8,64,64]{2,1,0:T(8,128)(2,1)} %param.23) | copy-start | bytes 196612
  18.1 8.4 %copy-start.5 = (f32[1024,8]{0,1:T(8,128)S(1)}, f32[1024,8]{0,1:T(8,128)}, u32[]{:S(2)}) copy-start(f32[1024,8]{0,1:T(8,128)} %param.25) | copy-start | bytes 98308
  18.1 72.0 %all-to-all-start = ((bf16[8,64,2048]{2,1,0:T(8,128)(2,1)}), bf16[8,64,2048]{2,1,0:T(8,128)(2,1)}, u32[]{:S(2)}, u32[]{:S(2)}) async-start(bf16[8,64,2048]{2,1,0:T(8,128)(2,1)} %bitcast.54), calls=%async_computation.1 | async-start | bytes 4194304 | tf_op jit(solution)/shard_map/all_to_all | solution.py:287
  25.5 1.1 copy-start.8
  25.6 1.2 copy-start.9
  25.6 199.5 %reduce-scatter.2.cloned.1.call-start = ((), (), s32[]{:S(2)}) async-start(), calls=%async_computation.4 | async-start | bytes 5242880 | tf_op jit(solution)/shard_map/reduce_scatter | solution.py:253
  49.4 5.3 %copy-start.11 = (bf16[1024,2048]{1,0:T(8,128)(2,1)S(1)}, bf16[1024,2048]{1,0:T(8,128)(2,1)}, u32[]{:S(2)}) copy-start(bf16[1024,2048]{1,0:T(8,128)(2,1)} %all-gather.8.cloned.1.call-done) | copy-start | bytes 12582916
  49.4 5.3 %copy-start.12 = (bf16[2048,512]{1,0:T(8,128)(2,1)S(1)}, bf16[2048,512]{1,0:T(8,128)(2,1)}, u32[]{:S(2)}) copy-start(bf16[2048,512]{1,0:T(8,128)(2,1)} %param.19) | copy-start | bytes 6291460
  158.5 4.1 %copy-start.1 = (bf16[1,1024,2048]{2,1,0:T(8,128)(2,1)S(1)}, bf16[1,1024,2048]{2,1,0:T(8,128)(2,1)}, u32[]{:S(2)}) copy-start(bf16[1,1024,2048]{2,1,0:T(8,128)(2,1)} %all-gather.14.cloned.1.call-done) | copy-start | bytes 12582916
  167.2 5.9 %copy-start.10 = (f32[128,2]{0,1:T(2,128)S(1)}, f32[128,2]{0,1:T(2,128)}, u32[]{:S(2)}) copy-start(f32[128,2]{0,1:T(2,128)} %param.30) | copy-start | bytes 3076
  167.2 54.4 %all-to-all-start.1 = ((bf16[8,64,2048]{2,1,0:T(8,128)(2,1)}), bf16[8,64,2048]{2,1,0:T(8,128)(2,1)}, u32[]{:S(2)}, u32[]{:S(2)}) async-start(bf16[8,64,2048]{2,1,0:T(8,128)(2,1)} %bitcast.53), calls=%async_computation.2 | async-start | bytes 4194304 | tf_op jit(solution)/shard_map/all_to_all | solution.py:313
Sparse Core Ops, SparseCore 0:
  12.2 37.1 all-gather.7
  51.0 34.9 all-gather.9
  87.6 34.9 all-gather.11
  124.0 34.4 all-gather.13
  161.5 44.5 reduce-scatter.1

commit v2 on v1

--- a/solution.py
+++ b/solution.py
@@ -6,6 +6,7 @@
 from jax.experimental import pallas as pl
 from jax.experimental.pallas import tpu as pltpu
 from jax.sharding import PartitionSpec as P
+
 
 epsilon = 1e-06
 gate_const = 8.0
@@ -223,7 +224,7 @@
     row_count, col_count = branch_x.shape
     groups = col_count // LANES
     plane = pltpu.VMEM((groups, row_count, LANES), jnp.float32)
-    mixed = pl.pallas_call(
+    call = pl.pallas_call(
         functools.partial(mixer_kernel, n),
         out_shape=jax.ShapeDtypeStruct((row_count, col_count), jnp.bfloat16),
         in_specs=[pl.BlockSpec(memory_space=pltpu.VMEM)] * 6,
@@ -249,13 +250,38 @@
             bytes_accessed=40 * row_count * col_count,
             transcendentals=6 * row_count * col_count,
         ),
-    )(branch_x, branch_gate, maps, conv_taps.astype(jnp.float32), slowness, decay_kick)
+    )
+    taps = conv_taps.astype(jnp.float32)
+    mixed = call(branch_x, branch_gate, maps, taps, slowness, decay_kick)
     return lax.psum_scatter(
         jnp.dot(mixed, w_mix_out, preferred_element_type=jnp.float32).astype(jnp.bfloat16),
         "tp",
         scatter_dimension=0,
         tiled=True,
     )
+
+
+def weight_pieces(own, axis):
+    size = lax.axis_size(axis)
+    pieces = [own]
+    if size & (size - 1):
+        for d in range(1, size):
+            route = [(i, (i + d) % size) for i in range(size)]
+            pieces.append(tuple(lax.ppermute(v, axis, route) for v in own))
+        return pieces
+    bit = size // 2
+    while bit:
+        route = [(i, i ^ bit) for i in range(size)]
+        sent = []
+        for piece in pieces:
+            moved = []
+            for v in piece:
+                moved.append(lax.ppermute(v, axis, route))
+            sent.append(tuple(moved))
+        pieces += sent
+        bit //= 2
+    order = [0] + [k for k in range(1, size) if k % 2 == 0] + [k for k in range(1, size) if k % 2]
+    return [pieces[k] for k in order]
 
 
 def run_experts(
@@ -288,27 +314,14 @@
     gate_mat = expert_gate_w[0]
     up_mat = expert_up_w[0]
     down_mat = expert_down_w[0]
-    full_gate, full_up, full_down = (
-        lax.all_gather(gate_mat, "tp", axis=1, tiled=True),
-        lax.all_gather(up_mat, "tp", axis=1, tiled=True),
-        lax.all_gather(down_mat, "tp", axis=0, tiled=True),
-    )
-    hidden = (
-        jax.nn.silu(jnp.dot(arrived, full_gate, preferred_element_type=jnp.float32))
-        * jnp.dot(arrived, full_up, preferred_element_type=jnp.float32)
-    ).astype(jnp.bfloat16)
-    groups = lax.axis_size("tp")
-    quarter = down_mat.shape[0]
-    summed_rows = jnp.zeros((arrived.shape[0], full_down.shape[1]), jnp.float32)
-    for group in range(groups):
-        piece = jnp.dot(
-            hidden[:, group * quarter : (group + 1) * quarter],
-            full_down[group * quarter : (group + 1) * quarter],
-            preferred_element_type=jnp.float32,
-        )
-        summed_rows = summed_rows + lax.optimization_barrier(piece.astype(jnp.bfloat16)).astype(
-            jnp.float32
-        )
+    width = gate_mat.shape[1]
+    pieces = weight_pieces((jnp.concatenate([gate_mat, up_mat], axis=1), down_mat), "tp")
+    summed_rows = None
+    for both_mat, down_piece in pieces:
+        pre = jnp.dot(arrived, both_mat, preferred_element_type=jnp.float32)
+        hidden = (jax.nn.silu(pre[:, :width]) * pre[:, width:]).astype(jnp.bfloat16)
+        part = jnp.dot(hidden, down_piece, preferred_element_type=jnp.float32)
+        summed_rows = part if summed_rows is None else summed_rows + part
     expert_done = summed_rows.astype(jnp.bfloat16)
     returned = lax.all_to_all(expert_done, "ep", split_axis=0, concat_axis=0, tiled=True)
     weighted_table = jnp.zeros((local_rows, slots_total), jnp.float32)
@@ -381,6 +394,7 @@
         P("ep", None, "tp"),
         P("ep", "tp", None),
     )
+
     return jax.shard_map(
         body,
         mesh=mesh,

time: 232 us -> 203 us (0.88)
  waiting for transfers between devices: 129 us -> 102 us
  Pallas kernels: 28.6 us -> 19.5 us
  matrix products: 35.6 us -> 39.8 us
  starting transfers between devices: 13.3 us -> 16.3 us
    all_gather x3 -> x0, waiting for transfers between devices: 56 us -> none  [the longest x1 30 us: run_experts(): lax.all_gather(down_mat, 'tp', axis=0, tiled=True)]
    all_gather x1, waiting for transfers between devices: 22.7 us -> 38.5 us  [run_mixer(): piece = lax.all_gather(mixer_in, 'tp', axis=0, tiled=True)]
    ppermute x0 -> x6, waiting for transfers between devices: none -> 15 us  [weight_pieces(): moved.append(lax.ppermute(v, axis, route))]
    pallas_call x1, Pallas kernels: 28.6 us -> 19.5 us  [run_mixer(): mixed = call(branch_x, branch_gate, maps, taps, slowness, decay_kick)]
    dot_general x6 -> x8, matrix products: 17.9 us -> 22 us  [the longest x4 13.9 us: run_experts(): pre = jnp.dot(arrived, both_mat, preferred_element_type=jnp.float32)]
    convert_element_type x2 -> x1, other arithmetic: 3.18 us -> 0.01 us  [run_mixer(): taps = conv_taps.astype(jnp.float32)]
    ppermute x0 -> x6, starting transfers between devices: none -> 3.1 us  [weight_pieces(): moved.append(lax.ppermute(v, axis, route))]
    concatenate x0 -> x1, other arithmetic: none -> 2.89 us  [run_experts(): jnp.concatenate([gate_mat, up_mat], axis=1)]
  transfers between devices with their start and end apart: 7 -> 10, of which waited for: 4 -> 3; matrix products, arithmetic and copies ran while one was open for 18% -> 22% of each run, Pallas kernels for 12% -> 10%
where the time goes in v2:
time: 203 us; the launch traced here: 202 us
  waiting for transfers between devices  102 us (50%)
  matrix products  39.8 us (20%)
  Pallas kernels  19.5 us (10%)
  starting transfers between devices  16.3 us (8%)
  between operations  14.4 us (7%)
  other arithmetic  8.81 us (4%)
    all_to_all x1, waiting for transfers between devices, run_experts(): lax.all_to_all(expert_done, 'ep', split_axis=0, concat_axis=0, tiled=True)  48.3 us
    all_gather x1, waiting for transfers between devices, run_mixer(): piece = lax.all_gather(mixer_in, 'tp', axis=0, tiled=True)  38.5 us
    pallas_call x1, Pallas kernels, run_mixer(): mixed = call(branch_x, branch_gate, maps, taps, slowness, decay_kick)  19.5 us
    ppermute x6, waiting for transfers between devices, weight_pieces(): moved.append(lax.ppermute(v, axis, route))  15 us
    dot_general x4, matrix products, run_experts(): pre = jnp.dot(arrived, both_mat, preferred_element_type=jnp.float32)  13.9 us
    dot_general x4, matrix products, run_experts(): part = jnp.dot(hidden, down_piece, preferred_element_type=jnp.float32)  8.13 us
    all_to_all x1, starting transfers between devices, run_experts(): lax.all_to_all(outgoing, 'ep', split_axis=0, concat_axis=0, tiled=True)  7.44 us
    all_to_all x1, starting transfers between devices, run_experts(): lax.all_to_all(expert_done, 'ep', split_axis=0, concat_axis=0, tiled=True)  5.66 us
  transfers between devices with their start and end apart: 10, of which 3 were waited for; matrix products, arithmetic and copies ran while one was open for 22% of the time, Pallas kernels for 10%

profile of v2, /device:TPU:0, one launch (start us, length us, event | category | flops | bytes accessed | tf_op | source)
XLA Modules:
  0.0 202.5 jit_solution(3281217098082577419)
XLA Ops:
  7.2 0.8 convert_element_type.77
  8.1 1.6 fusion
  9.6 2.5 %fusion.2 = bf16[256,2048]{1,0:T(8,128)(2,1)} fusion(bf16[256,2048]{1,0:T(8,128)(2,1)} %param.17, f32[2048]{0:T(1024)S(1)} %convert_element_type.77, f32[256]{0:T(256)S(1)} %add_rsqrt_fusion), kind=kLoop, calls=%fused_computation.8 | loop fusion | flops 2097152 | bytes 2106368 | tf_op jit(solution)/shard_map/convert_element_type | solution.py:18
  13.7 2.4 %convolution_convert_fusion.1 = bf16[512,2048]{1,0:T(8,128)(2,1)} fusion(bf16[128,2048]{1,0:T(8,128)(2,1)S(1)} %copy-done.1, f32[2048]{0:T(1024)S(1)} %convert_element_type.88, f32[128]{0:T(128)S(1)} %add_rsqrt_fusion.1, s32[256]{0:T(256)S(1)} %get-tuple-element.9, s32[256]{0:T(256)S(1)} %get-tuple-element.8), kind=kOutput, calls=%fused_computation.2 | convolution fusion | flops 304316416 | bytes 2632192 | tf_op jit(solution)/shard_map/dot_general | solution.py:310
  16.1 7.4 %all-to-all-start = ((bf16[8,64,2048]{2,1,0:T(8,128)(2,1)}), bf16[8,64,2048]{2,1,0:T(8,128)(2,1)}, u32[]{:S(2)}, u32[]{:S(2)}) async-start(bf16[8,64,2048]{2,1,0:T(8,128)(2,1)} %bitcast.46), calls=%async_computation.1 | async-start | bytes 4194304 | tf_op jit(solution)/shard_map/all_to_all | solution.py:313
  23.7 2.9 %pad_maximum_fusion = bf16[2048,512]{1,0:T(8,128)(2,1)} fusion(bf16[2048,256]{1,0:T(8,128)(2,1)S(1)} %bitcast.49, bf16[2048,256]{1,0:T(8,128)(2,1)} %bitcast.50), kind=kLoop, calls=%fused_computation.9 | loop fusion | flops 4194304 | bytes 4194304 | tf_op jit(solution)/shard_map/concatenate | solution.py:318
  26.6 1.8 collective-permute-start.2
  29.8 38.5 %all-gather.2.cloned.1.call-done = bf16[1024,2048]{1,0:T(8,128)(2,1)} async-done(((bf16[256,2048]{1,0:T(8,128)(2,1)}), bf16[1024,2048]{1,0:T(8,128)(2,1)}) %all-gather.2.cloned.1.call-update) | async-done | bytes 4194320 | tf_op jit(solution)/shard_map/all_gather | solution.py:216
  68.3 5.3 %convolution_convert_fusion.3.gate_ref = bf16[1024,512]{1,0:T(8,128)(2,1)S(1)} fusion(bf16[1024,2048]{1,0:T(8,128)(2,1)} %all-gather.2.cloned.1.call-done, bf16[2048,512]{1,0:T(8,128)(2,1)} %param.20), kind=kOutput, calls=%fused_computation.10 | convolution fusion | flops 2148007936 | bytes 7340032 | tf_op jit(solution)/shard_map/dot_general | solution.py:218
  73.6 2.3 %convolution_convert_fusion.4.x_ref = bf16[1024,512]{1,0:T(8,128)(2,1)S(1)} fusion(bf16[1024,2048]{1,0:T(8,128)(2,1)S(1)} %copy-done.11, bf16[2048,512]{1,0:T(8,128)(2,1)S(1)} %copy-done.12), kind=kOutput, calls=%fused_computation.11 | convolution fusion | flops 2148007936 | bytes 7340032 | tf_op jit(solution)/shard_map/dot_general | solution.py:217
  75.9 19.5 %shard_map.176 = bf16[1024,512]{1,0:T(8,128)(2,1)S(1)} custom-call(bf16[1024,512]{1,0:T(8,128)(2,1)S(1)} %convolution_convert_fusion.4.x_ref, bf16[1024,512]{1,0:T(8,128)(2,1)S(1)} %convolution_convert_fusion.3.gate_ref, bf16[4,128,256]{2,1,0:T(8,128)(2,1)S(1)} %pad_maximum_fusion.1.maps_ref, f32[4,512]{1,0:T(4,128)S(1)} %convert_element_type.82.taps_ref, ...), custom_call_target="tpu_custom_call" | custom-call | flops 52428800 | bytes 20971520 | tf_op jit(solution)/shard_map/pallas_call | solution.py:255
  95.5 4.3 %convolution_convert_fusion = bf16[1024,2048]{1,0:T(8,128)(2,1)} fusion(bf16[1024,512]{1,0:T(8,128)(2,1)S(1)} %shard_map.176, bf16[512,2048]{1,0:T(8,128)(2,1)S(1)} %copy-done), kind=kOutput, calls=%fused_computation.1 | convolution fusion | flops 2149580800 | bytes 7340032 | tf_op jit(solution)/shard_map/dot_general | solution.py:257
  100.4 15.0 %collective-permute-done.3 = bf16[256,2048]{1,0:T(8,128)(2,1)} collective-permute-done((bf16[256,2048]{1,0:T(8,128)(2,1)}, bf16[256,2048]{1,0:T(8,128)(2,1)}, u32[]{:S(2)}, u32[]{:S(2)}) %collective-permute-start.3) | collective-permute-done | bytes 1048608 | tf_op jit(solution)/shard_map/ppermute | solution.py:279
  115.9 3.4 %fusion.45 = f32[512,512]{1,0:T(8,128)S(1)} fusion(bf16[512,2048]{1,0:T(8,128)(2,1)} %bitcast.10, bf16[2048,256]{1,0:T(8,128)(2,1)} %bitcast.48, bf16[2048,256]{1,0:T(8,128)(2,1)} %bitcast.51), kind=kOutput, calls=%fused_computation.79 | convolution fusion | flops 1077936128 | bytes 5242880 | tf_op jit(solution)/shard_map/dot_general | solution.py:321
  119.3 3.5 %fusion.47 = f32[512,512]{1,0:T(8,128)S(1)} fusion(bf16[512,2048]{1,0:T(8,128)(2,1)} %bitcast.10, bf16[2048,512]{1,0:T(8,128)(2,1)} %collective-permute-done.2), kind=kOutput, calls=%fused_computation.81 | convolution fusion | flops 1073741824 | bytes 5242880 | tf_op jit(solution)/shard_map/dot_general | solution.py:321
  122.8 2.0 fusion.13
  124.8 3.5 %fusion.46 = f32[512,512]{1,0:T(8,128)S(1)} fusion(bf16[512,2048]{1,0:T(8,128)(2,1)} %bitcast.10, bf16[2048,512]{1,0:T(8,128)(2,1)} %collective-permute-done), kind=kOutput, calls=%fused_computation.80 | convolution fusion | flops 1073741824 | bytes 5242880 | tf_op jit(solution)/shard_map/dot_general | solution.py:321
  128.3 2.0 fusion.17
  130.2 2.0 fusion.15
  132.2 3.6 %fusion.48 = f32[512,512]{1,0:T(8,128)S(1)} fusion(bf16[512,2048]{1,0:T(8,128)(2,1)} %bitcast.10, bf16[2048,512]{1,0:T(8,128)(2,1)} %collective-permute-done.4), kind=kOutput, calls=%fused_computation.82 | convolution fusion | flops 1073741824 | bytes 5242880 | tf_op jit(solution)/shard_map/dot_general | solution.py:321
  135.8 2.2 %add_convert_fusion = bf16[512,2048]{1,0:T(8,128)(2,1)} fusion(f32[512,2048]{1,0:T(8,128)S(1)} %fusion.17, f32[512,2048]{1,0:T(8,128)S(1)} %fusion.13, f32[512,2048]{1,0:T(8,128)S(1)} %fusion.15, bf16[256,2048]{1,0:T(8,128)(2,1)S(1)} %collective-permute-done.5, f32[512,512]{1,0:T(8,128)S(1)} %fusion.48), kind=kOutput, calls=%fused_computation | convolution fusion | flops 541851648 | bytes 16777216 | tf_op jit(solution)/shard_map/dot_general | solution.py:323
  138.0 5.7 %all-to-all-start.1 = ((bf16[8,64,2048]{2,1,0:T(8,128)(2,1)}), bf16[8,64,2048]{2,1,0:T(8,128)(2,1)}, u32[]{:S(2)}, u32[]{:S(2)}) async-start(bf16[8,64,2048]{2,1,0:T(8,128)(2,1)} %bitcast.47), calls=%async_computation.2 | async-start | bytes 4194304 | tf_op jit(solution)/shard_map/all_to_all | solution.py:326
  143.9 48.3 %all-to-all-done.1 = bf16[8,64,2048]{2,1,0:T(8,128)(2,1)} async-done(((bf16[8,64,2048]{2,1,0:T(8,128)(2,1)}), bf16[8,64,2048]{2,1,0:T(8,128)(2,1)}, u32[]{:S(2)}, u32[]{:S(2)}) %all-to-all-start.1) | async-done | bytes 2097184 | tf_op jit(solution)/shard_map/all_to_all | solution.py:326
  192.2 3.4 %convolution_convert_fusion.2 = bf16[128,2048]{1,0:T(8,128)(2,1)} fusion(bf16[512,2048]{1,0:T(8,128)(2,1)} %bitcast.15, f32[128]{0:T(128)S(1)} %get-tuple-element.7, s32[128]{0:T(128)S(1)} %get-tuple-element.5, f32[128]{0:T(128)S(1)} %get-tuple-element.6, s32[128]{0:T(128)S(1)} %get-tuple-element.4), kind=kOutput, calls=%fused_computation.5 | convolution fusion | flops 1611202560 | bytes 2623488 | tf_op jit(solution)/shard_map/dot_general | solution.py:334
  (73 shorter events, 4.3 us)
Async XLA Ops:
  7.2 88.3 %copy-start = (bf16[512,2048]{1,0:T(8,128)(2,1)S(1)}, bf16[512,2048]{1,0:T(8,128)(2,1)}, u32[]{:S(2)}) copy-start(bf16[512,2048]{1,0:T(8,128)(2,1)} %param.26) | copy-start | bytes 6291460
  7.2 61.1 %all-gather.2.cloned.1.call-start = ((), (), s32[]{:S(2)}) async-start(), calls=%async_computation.3 | async-start | bytes 5242880 | tf_op jit(solution)/shard_map/all_gather | solution.py:216
  8.1 4.1 %copy-start.6 = (s32[128,2]{0,1:T(2,128)S(1)}, s32[128,2]{0,1:T(2,128)}, u32[]{:S(2)}) copy-start(s32[128,2]{0,1:T(2,128)} %param.29) | copy-start | bytes 3076
  8.1 5.4 %copy-start.7 = (bf16[2048]{0:T(1024)(128)(2,1)S(1)}, bf16[2048]{0:T(1024)(128)(2,1)}, u32[]{:S(2)}) copy-start(bf16[2048]{0:T(1024)(128)(2,1)} %param.28) | copy-start | bytes 12292
  8.1 5.5 %copy-start.1 = (bf16[128,2048]{1,0:T(8,128)(2,1)S(1)}, bf16[128,2048]{1,0:T(8,128)(2,1)}, u32[]{:S(2)}) copy-start(bf16[128,2048]{1,0:T(8,128)(2,1)} %param.27) | copy-start | bytes 1572868
  16.1 7.5 %copy-start.2 = (bf16[1,2048,256]{2,1,0:T(8,128)(2,1)S(1)}, bf16[1,2048,256]{2,1,0:T(8,128)(2,1)}, u32[]{:S(2)}) copy-start(bf16[1,2048,256]{2,1,0:T(8,128)(2,1)} %param.32) | copy-start | bytes 3145732
  16.1 99.8 %all-to-all-start = ((bf16[8,64,2048]{2,1,0:T(8,128)(2,1)}), bf16[8,64,2048]{2,1,0:T(8,128)(2,1)}, u32[]{:S(2)}, u32[]{:S(2)}) async-start(bf16[8,64,2048]{2,1,0:T(8,128)(2,1)} %bitcast.46), calls=%async_computation.1 | async-start | bytes 4194304 | tf_op jit(solution)/shard_map/all_to_all | solution.py:313
  23.6 172.1 %reduce-scatter.2.cloned.1.call-start = ((), (), s32[]{:S(2)}) async-start(), calls=%async_computation.4 | async-start | bytes 5242880 | tf_op jit(solution)/shard_map/reduce_scatter | solution.py:256
  23.6 5.0 %copy-start.3 = (bf16[8,64,64]{2,1,0:T(8,128)(2,1)S(1)}, bf16[8,64,64]{2,1,0:T(8,128)(2,1)}, u32[]{:S(2)}) copy-start(bf16[8,64,64]{2,1,0:T(8,128)(2,1)} %param.22) | copy-start | bytes 196612
  23.7 5.2 %copy-start.4 = (bf16[8,64,64]{2,1,0:T(8,128)(2,1)S(1)}, bf16[8,64,64]{2,1,0:T(8,128)(2,1)}, u32[]{:S(2)}) copy-start(bf16[8,64,64]{2,1,0:T(8,128)(2,1)} %param.23) | copy-start | bytes 196612
  23.7 5.8 %copy-start.5 = (f32[1024,8]{0,1:T(8,128)S(1)}, f32[1024,8]{0,1:T(8,128)}, u32[]{:S(2)}) copy-start(f32[1024,8]{0,1:T(8,128)} %param.25) | copy-start | bytes 98308
  26.6 3.1 %copy-start.8 = (bf16[4,512]{1,0:T(4,128)(2,1)S(1)}, bf16[4,512]{1,0:T(4,128)(2,1)}, u32[]{:S(2)}) copy-start(bf16[4,512]{1,0:T(4,128)(2,1)} %param.21) | copy-start | bytes 12292
  26.6 3.2 %copy-start.9 = (f32[512]{0:T(512)S(1)}, f32[512]{0:T(512)}, u32[]{:S(2)}) copy-start(f32[512]{0:T(512)} %param.24) | copy-start | bytes 6148
  26.6 88.8 %collective-permute-start.2 = (bf16[2048,512]{1,0:T(8,128)(2,1)}, bf16[2048,512]{1,0:T(8,128)(2,1)}, u32[]{:S(2)}, u32[]{:S(2)}) collective-permute-start(bf16[2048,512]{1,0:T(8,128)(2,1)} %pad_maximum_fusion), channel_id=1, source_target_pairs={{0,2},{1,3},{2,0},{3,1},{4,6},{5,7},{6,4},{7,5},{8,10},{9,11},{10,... | collective-permute-start | bytes 6291464 | tf_op jit(solution)/shard_map/ppermute | solution.py:279
  28.3 87.1 %collective-permute-start.3 = (bf16[256,2048]{1,0:T(8,128)(2,1)}, bf16[256,2048]{1,0:T(8,128)(2,1)}, u32[]{:S(2)}, u32[]{:S(2)}) collective-permute-start(bf16[256,2048]{1,0:T(8,128)(2,1)} %bitcast.13), channel_id=1, source_target_pairs={{0,2},{1,3},{2,0},{3,1},{4,6},{5,7},{6,4},{7,5},{8,10},{9,11},{10,... | collective-permute-start | bytes 3145736 | tf_op jit(solution)/shard_map/ppermute | solution.py:279
  68.3 5.3 %copy-start.11 = (bf16[1024,2048]{1,0:T(8,128)(2,1)S(1)}, bf16[1024,2048]{1,0:T(8,128)(2,1)}, u32[]{:S(2)}) copy-start(bf16[1024,2048]{1,0:T(8,128)(2,1)} %all-gather.2.cloned.1.call-done) | copy-start | bytes 12582916
  68.3 5.3 %copy-start.12 = (bf16[2048,512]{1,0:T(8,128)(2,1)S(1)}, bf16[2048,512]{1,0:T(8,128)(2,1)}, u32[]{:S(2)}) copy-start(bf16[2048,512]{1,0:T(8,128)(2,1)} %param.19) | copy-start | bytes 6291460
  99.8 25.0 %collective-permute-start = (bf16[2048,512]{1,0:T(8,128)(2,1)}, bf16[2048,512]{1,0:T(8,128)(2,1)}, u32[]{:S(2)}, u32[]{:S(2)}) collective-permute-start(bf16[2048,512]{1,0:T(8,128)(2,1)} %pad_maximum_fusion), channel_id=1, source_target_pairs={{0,1},{1,0},{2,3},{3,2},{4,5},{5,4},{6,7},{7,6},{8,9},{9,8},{10,11... | collective-permute-start | bytes 6291464 | tf_op jit(solution)/shard_map/ppermute | solution.py:279
  99.9 30.3 %collective-permute-start.1 = (bf16[256,2048]{1,0:T(8,128)(2,1)}, bf16[256,2048]{1,0:T(8,128)(2,1)}, u32[]{:S(2)}, u32[]{:S(2)}) collective-permute-start(bf16[256,2048]{1,0:T(8,128)(2,1)} %bitcast.13), channel_id=1, source_target_pairs={{0,1},{1,0},{2,3},{3,2},{4,5},{5,4},{6,7},{7,6},{8,9},{9,8},{10,11... | collective-permute-start | bytes 3145736 | tf_op jit(solution)/shard_map/ppermute | solution.py:279
  115.4 20.4 %collective-permute-start.5 = (bf16[256,2048]{1,0:T(8,128)(2,1)}, bf16[256,2048]{1,0:T(8,128)(2,1)S(1)}, u32[]{:S(2)}, u32[]{:S(2)}) collective-permute-start(bf16[256,2048]{1,0:T(8,128)(2,1)} %collective-permute-done.3), channel_id=1, source_target_pairs={{0,1},{1,0},{2,3},{3,2},{4,5},{5,4},{6,7},{7,6},{8,9},{9,8},{10,11... | collective-permute-start | bytes 3145736 | tf_op jit(solution)/shard_map/ppermute | solution.py:279
  115.4 16.8 %collective-permute-start.4 = (bf16[2048,512]{1,0:T(8,128)(2,1)}, bf16[2048,512]{1,0:T(8,128)(2,1)}, u32[]{:S(2)}, u32[]{:S(2)}) collective-permute-start(bf16[2048,512]{1,0:T(8,128)(2,1)} %collective-permute-done.2), channel_id=1, source_target_pairs={{0,1},{1,0},{2,3},{3,2},{4,5},{5,4},{6,7},{7,6},{8,9},{9,8},{10,11... | collective-permute-start | bytes 6291464 | tf_op jit(solution)/shard_map/ppermute | solution.py:279
  138.0 5.9 %copy-start.10 = (f32[128,2]{0,1:T(2,128)S(1)}, f32[128,2]{0,1:T(2,128)}, u32[]{:S(2)}) copy-start(f32[128,2]{0,1:T(2,128)} %param.30) | copy-start | bytes 3076
  138.0 54.2 %all-to-all-start.1 = ((bf16[8,64,2048]{2,1,0:T(8,128)(2,1)}), bf16[8,64,2048]{2,1,0:T(8,128)(2,1)}, u32[]{:S(2)}, u32[]{:S(2)}) async-start(bf16[8,64,2048]{2,1,0:T(8,128)(2,1)} %bitcast.47), calls=%async_computation.2 | async-start | bytes 4194304 | tf_op jit(solution)/shard_map/all_to_all | solution.py:326
Sparse Core Ops, SparseCore 0:
  12.3 55.9 all-gather.1
  99.9 44.3 reduce-scatter.1
